TPU v7x, 32 devices: a whole 2x2x4 slice. The times are simulated.
32 devices in a mesh: fs: 8 (over z, y), tp: 4 (over x, core).
Axes of the slice: x: 2, y: 2, z: 4, core: 2. Of those that a mesh axis runs over, the one named last changes fastest.
Arguments:
- inputs: bfloat16 [48, 4096], P('fs', 'tp'), may hold values from -0.875 to 0.875
- cotangent: bfloat16 [48, 4096], P('fs', 'tp'), may hold values from -8 to 8
- pre_act: bfloat16 [48, 16384], P(None, 'fs'), may hold values from -3 to 3
- w_up: bfloat16 [4096, 16384], P('tp', 'fs'), may hold values from -0.046875 to 0.046875
- w_down: bfloat16 [16384, 4096], P('fs', 'tp'), may hold values from -0.09375 to 0.09375
Outputs:
- grad_input: bfloat16 [48, 4096], P('fs', 'tp')
- grad_up: float32 [4096, 16384], P('tp', 'fs')
- grad_down: float32 [16384, 4096], P('fs', 'tp')
All inputs are finite; a program needn't handle non-finite values.
Results may differ from a plain program's by a relative error of at most 0.017.
Values may be sent and summed in bfloat16 or wider, within the bound.
A program may use at most 64 MiB of HBM per device.

v0:
```python
import functools

import jax
import jax.numpy as jnp
from jax import lax
from jax.experimental import pallas as pl
from jax.experimental.pallas import tpu as pltpu
from jax.sharding import PartitionSpec as P

F32, BF16 = jnp.float32, jnp.bfloat16
SLAB = 8
NT = (((1,), (1,)), ((), ()))
TN = (((0,), (0,)), ((), ()))
NN = (((1,), (0,)), ((), ()))


def dot(a, b, dims):
    return lax.dot_general(a, b, dims, preferred_element_type=F32)


def exchange(
    n,
    chips,
    chunks,
    cot_ref,
    in_ref,
    pre_ref,
    wu_ref,
    wd_ref,
    cot_out,
    in_out,
    act_out,
    gp_out,
    gi_out,
    cot_v,
    in_v,
    pre_v,
    wu_v,
    wd_v,
    cot_g,
    in_g,
    spread,
    own,
    p1_s,
    p1_r,
    p2_s,
    p2_r,
    rs_s,
    rs_r,
    local,
    cs,
    cr,
    is_,
    ir,
    s1,
    r1,
    s2,
    r2,
    s3,
    r3,
    s4,
    r4,
):
    me = lax.axis_index("fs")
    tp = lax.axis_index("tp")
    core = lax.rem(tp, 2)
    rows = cot_v.shape[0]
    tokens = n * rows
    width = wd_v.shape[1]
    fs_peer = [None] + [lax.rem(me + k, n) for k in range(1, n)]
    partner = tp + 1 - 2 * core
    x_peer = [None] + [lax.rem(tp + 2 * k, 2 * chips) for k in range(1, chips)]
    targets = (
        [{"fs": p} for p in fs_peer[1:]]
        + [{"tp": partner}]
        + [{"tp": p} for p in x_peer[1:]]
    )

    barrier = pltpu.get_barrier_semaphore()
    for t in targets:
        pl.semaphore_signal(barrier, inc=1, device_id=t)

    load_cot = pltpu.make_async_copy(cot_ref, cot_v, local.at[0])
    load_in = pltpu.make_async_copy(in_ref, in_v, local.at[1])
    load_cot.start()
    load_in.start()
    load_wd, load_pre, load_wu = [], [], []
    for j in range(2 * chunks):
        load_wd.append(
            pltpu.make_async_copy(
                wd_ref.at[pl.ds(j * width, width)], wd_v.at[j], local.at[4 + j]
            )
        )
        load_wd[-1].start()
    for j in range(2 * chunks):
        load_pre.append(
            pltpu.make_async_copy(
                pre_ref.at[:, pl.ds(j * width, width)],
                pre_v.at[j],
                local.at[4 + 2 * chunks + j],
            )
        )
        load_pre[-1].start()
    for j in range(2 * chunks):
        load_wu.append(
            pltpu.make_async_copy(
                wu_ref.at[:, pl.ds(j * width, width)],
                wu_v.at[j],
                local.at[4 + 4 * chunks + j],
            )
        )
        load_wu[-1].start()
    spread[...] = jnp.zeros_like(spread)
    load_cot.wait()
    load_in.wait()
    own_cot = pltpu.make_async_copy(cot_v, cot_g.at[me], local.at[2])
    own_in = pltpu.make_async_copy(in_v, in_g.at[me], local.at[3])
    own_cot.start()
    own_in.start()

    pl.semaphore_wait(barrier, len(targets))
    sends_c, sends_i = [], []
    for k in range(1, n):
        copy = pltpu.make_async_remote_copy(
            cot_v, cot_g.at[me], cs.at[k], cr.at[k], device_id={"fs": fs_peer[k]}
        )
        copy.start()
        sends_c.append(copy)
    def picker(shape, token_dim):
        t = lax.broadcasted_iota(jnp.int32, shape, token_dim)
        j = lax.broadcasted_iota(jnp.int32, shape, 1 - token_dim)
        q, r = j // SLAB, j % SLAB
        return ((t == q * rows + r) & (r < rows)).astype(F32).astype(BF16)

    pick = picker((tokens, n * SLAB), 0)
    place = picker((n * SLAB, tokens), 1)

    def gathered(ref):
        for s in range(n):
            spread[s * SLAB : s * SLAB + rows, :] = ref[s].astype(F32)
        return dot(pick, spread[...].astype(BF16), NN).astype(BF16)

    own_cot.wait()
    for copy in load_wd:
        copy.wait()
    for copy in sends_c:
        copy.wait_recv()
    cot_out[...] = gathered(cot_g)

    first, other = core * chunks, (1 - core) * chunks
    send1, send2 = [], []

    def to_partner(j):
        p1_s[j] = dot(cot_out[...], wd_v[other + j], NT).astype(BF16)
        copy = pltpu.make_async_remote_copy(
            p1_s.at[j], p1_r.at[j], s1.at[j], r1.at[j], device_id={"tp": partner}
        )
        copy.start()
        send1.append(copy)

    def to_chips(j):
        send1[j].wait_recv()
        total = own[j] + p1_r[j].astype(F32)
        own[j] = total
        p2_s[j] = total.astype(BF16)
        for k in range(1, chips):
            copy = pltpu.make_async_remote_copy(
                p2_s.at[j],
                p2_r.at[k - 1, j],
                s2.at[k - 1, j],
                r2.at[k - 1, j],
                device_id={"tp": x_peer[k]},
            )
            copy.start()
            send2.append(copy)

    to_partner(0)
    for k in range(1, n):
        copy = pltpu.make_async_remote_copy(
            in_v, in_g.at[me], is_.at[k], ir.at[k], device_id={"fs": fs_peer[k]}
        )
        copy.start()
        sends_i.append(copy)
    for j in range(chunks):
        own[j] = dot(cot_out[...], wd_v[first + j], NT)
        if j + 1 < chunks:
            to_partner(j + 1)
        to_chips(j)

    own_in.wait()
    for copy in sends_i:
        copy.wait_recv()
    in_out[...] = gathered(in_g)
    for copy in load_pre:
        copy.wait()
    for j in range(2 * chunks):
        active = jnp.maximum(pre_v[j].astype(F32), 0.0)
        act_out[j] = (active * active).astype(BF16)
    for copy in load_wu:
        copy.wait()

    send3 = []
    for j in range(chunks):
        hidden = own[j]
        for k in range(1, chips):
            send2[j * (chips - 1) + k - 1].wait_recv()
            hidden = hidden + p2_r[k - 1, j].astype(F32)
        active = jnp.maximum(pre_v[first + j].astype(F32), 0.0)
        gp_out[first + j] = (2.0 * active * hidden).astype(BF16)
        copy = pltpu.make_async_remote_copy(
            gp_out.at[first + j],
            gp_out.at[first + j],
            s3.at[j],
            r3.at[j],
            device_id={"tp": partner},
        )
        copy.start()
        send3.append(copy)
    acc = None
    for j in range(chunks):
        term = dot(gp_out[first + j], wu_v[first + j], NT)
        acc = term if acc is None else acc + term
    for j in range(chunks):
        pltpu.make_async_remote_copy(
            gp_out.at[other + j],
            gp_out.at[other + j],
            s3.at[j],
            r3.at[j],
            device_id={"tp": partner},
        ).wait_recv()
        acc = acc + dot(gp_out[other + j], wu_v[other + j], NT)
    slabs = dot(place, acc.astype(BF16), NN)
    for s in range(n):
        rs_s[s] = slabs[s * SLAB : s * SLAB + rows, :].astype(BF16)
    send4 = []
    for k in range(1, n):
        copy = pltpu.make_async_remote_copy(
            rs_s.at[fs_peer[k]],
            rs_r.at[k - 1],
            s4.at[k],
            r4.at[k],
            device_id={"fs": fs_peer[k]},
        )
        copy.start()
        send4.append(copy)
    for copy in sends_c + sends_i + send1 + send2 + send3:
        copy.wait_send()
    total = rs_s[me].astype(F32)
    for k in range(1, n):
        send4[k - 1].wait_recv()
        total = total + rs_r[k - 1].astype(F32)
    gi_out[...] = total.astype(BF16)
    for copy in send4:
        copy.wait_send()


def outer(
    chunks, cot_v, in_v, act_v, gp_v, gi_v, gi_out, gu_out, gd_out, gu_v, gd_v, sem
):
    width = gp_v.shape[2]
    pieces = []

    def put(src, dst):
        copy = pltpu.make_async_copy(src, dst, sem.at[len(pieces)])
        copy.start()
        pieces.append(copy)

    half = width // 2
    for j in range(2 * chunks):
        for h in range(2):
            rows = pl.ds(j * width + h * half, half)
            gd_v[rows, :] = dot(act_v[j, :, h * half : (h + 1) * half], cot_v[...], TN)
            put(gd_v.at[rows], gd_out.at[rows])
    put(gi_v, gi_out)
    step = in_v.shape[1] // (4 * chunks)
    for i in range(4 * chunks):
        rows = pl.ds(i * step, step)
        for j in range(2 * chunks):
            gu_v[rows, j * width : (j + 1) * width] = dot(
                in_v[:, i * step : (i + 1) * step], gp_v[j], TN
            )
        put(gu_v.at[rows], gu_out.at[rows])
    for copy in pieces:
        copy.wait()


def fused(n, ntp, inputs, cotangent, pre_act, w_up, w_down):
    rows, d = inputs.shape
    tokens, ff = pre_act.shape
    chips = ntp // 2
    chunks = 2 if (ff // 2) % 256 == 0 else 1
    width = ff // 2 // chunks
    hbm = pl.BlockSpec(memory_space=pl.ANY)
    vmem = pl.BlockSpec(memory_space=pltpu.VMEM)
    dma = pltpu.SemaphoreType.DMA
    cot, full, act, gp, gi = pl.pallas_call(
        functools.partial(exchange, n, chips, chunks),
        out_shape=(
            pltpu.VMEM((tokens, d), BF16),
            pltpu.VMEM((tokens, d), BF16),
            pltpu.VMEM((2 * chunks, tokens, width), BF16),
            pltpu.VMEM((2 * chunks, tokens, width), BF16),
            pltpu.VMEM((rows, d), BF16),
        ),
        in_specs=[hbm] * 5,
        out_specs=(vmem,) * 5,
        scratch_shapes=[
            pltpu.VMEM((rows, d), BF16),
            pltpu.VMEM((rows, d), BF16),
            pltpu.VMEM((2 * chunks, tokens, width), BF16),
            pltpu.VMEM((2 * chunks, d, width), BF16),
            pltpu.VMEM((2 * chunks, width, d), BF16),
            pltpu.VMEM((n, rows, d), BF16),
            pltpu.VMEM((n, rows, d), BF16),
            pltpu.VMEM((n * SLAB, d), F32),
            pltpu.VMEM((chunks, tokens, width), F32),
            pltpu.VMEM((chunks, tokens, width), BF16),
            pltpu.VMEM((chunks, tokens, width), BF16),
            pltpu.VMEM((chunks, tokens, width), BF16),
            pltpu.VMEM((chips - 1, chunks, tokens, width), BF16),
            pltpu.VMEM((n, rows, d), BF16),
            pltpu.VMEM((n - 1, rows, d), BF16),
            dma((4 + 6 * chunks,)),
            dma((n,)),
            dma((n,)),
            dma((n,)),
            dma((n,)),
            dma((chunks,)),
            dma((chunks,)),
            dma((chips - 1, chunks)),
            dma((chips - 1, chunks)),
            dma((chunks,)),
            dma((chunks,)),
            dma((n,)),
            dma((n,)),
        ],
        compiler_params=pltpu.CompilerParams(collective_id=0, has_side_effects=True),
    )(cotangent, inputs, pre_act, w_up, w_down)
    return pl.pallas_call(
        functools.partial(outer, chunks),
        out_shape=(
            jax.ShapeDtypeStruct((rows, d), BF16),
            jax.ShapeDtypeStruct((d, ff), F32),
            jax.ShapeDtypeStruct((ff, d), F32),
        ),
        in_specs=[vmem] * 5,
        out_specs=(hbm,) * 3,
        scratch_shapes=[
            pltpu.VMEM((d, ff), F32),
            pltpu.VMEM((ff, d), F32),
            dma((8 * chunks + 1,)),
        ],
    )(*(pltpu.with_memory_space_constraint(x, pltpu.VMEM) for x in (cot, full, act, gp, gi)))


def plain(inputs, cotangent, pre_act, w_up, w_down):
    active = jax.nn.relu(pre_act.astype(F32))
    squared = jnp.square(active).astype(BF16)
    piece = lax.all_gather(cotangent, "fs", axis=0, tiled=True)
    grad_down = dot(squared, piece, TN)
    hidden = lax.psum(dot(piece, w_down, NT).astype(BF16), "tp").astype(F32)
    grad_pre = (2.0 * active * hidden).astype(BF16)
    grad_up = dot(lax.all_gather(inputs, "fs", axis=0, tiled=True), grad_pre, TN)
    grad_input = lax.psum_scatter(
        dot(grad_pre, w_up, NT), "fs", scatter_dimension=0, tiled=True
    ).astype(BF16)
    return (grad_input, grad_up, grad_down)


def solution(mesh):
    n, ntp = mesh.shape["fs"], mesh.shape["tp"]

    def body(inputs, cotangent, pre_act, w_up, w_down):
        rows, d = inputs.shape
        tokens, ff = pre_act.shape
        if (
            1 < n <= 16
            and ntp > 2
            and ntp % 2 == 0
            and rows <= SLAB
            and tokens % 16 == 0
            and d % 1024 == 0
            and ff % 1024 == 0
        ):
            return fused(n, ntp, inputs, cotangent, pre_act, w_up, w_down)
        return plain(inputs, cotangent, pre_act, w_up, w_down)

    return jax.shard_map(
        body,
        mesh=mesh,
        in_specs=(P("fs", "tp"), P("fs", "tp"), P(None, "fs"), P("tp", "fs"), P("fs", "tp")),
        out_specs=(P("fs", "tp"), P("tp", "fs"), P("fs", "tp")),
        check_vma=False,
    )
```

profile of v0, /device:TPU:0, one launch (start us, length us, event | category | flops | bytes accessed | tf_op | source)
XLA Modules:
  0.0 30.8 jit_solution(6082693231599375201)
XLA Ops:
  0.6 23.9 %shard_map.76 = (bf16[48,1024]{1,0:T(8,128)(2,1)S(1)}, bf16[48,1024]{1,0:T(8,128)(2,1)S(1)}, bf16[4,48,512]{2,1,0:T(8,128)(2,1)S(1)}, bf16[4,48,512]{2,1,0:T(8,128)(2,1)S(1)}, bf16[6,1024]{1,0:T(8,128)(2,1)S(1)}) custom-call(bf16[6,1024]{1,0:T(8,128)(2,1)} %cot_ref.1, bf16[6,1024]{1,0:T(8,128)(2,1)} %in_ref.1, bf16[48,2048]{1,0:T(8,128)(2,1)} %pre_ref.1, ...), custom_call_target="tpu_custom_call" | custom-call | tf_op jit(solution)/shard_map/pallas_call | solution.py:296
  24.5 6.3 %shard_map.77 = (bf16[6,1024]{1,0:T(8,128)(2,1)}, f32[1024,2048]{1,0:T(8,128)}, f32[2048,1024]{1,0:T(8,128)}) custom-call(bf16[48,1024]{1,0:T(8,128)(2,1)S(1)} %get-tuple-element.8.cot_v, bf16[48,1024]{1,0:T(8,128)(2,1)S(1)} %get-tuple-element.9.in_v, bf16[4,48,512]{2,1,0:T(8,128)(2,1)S(1)} %get-tuple-element.10.act_v, ...), custom_call_target="tpu_custom_call" | custom-call | tf_op jit(solution)/shard_map/pallas_call | solution.py:339
where the time goes:
time: 31.1 us; the launch traced here: 30.8 us
  Pallas kernels  30.2 us (97%)
  between operations  0.64 us (2%)
    pallas_call x1, Pallas kernels, fused(): pl.pallas_call(functools.partial(exchange, n, chips, chunks), out_shape=(...  23.9 us
    pallas_call x1, Pallas kernels, fused(): pl.pallas_call(functools.partial(outer, chunks), out_shape=(jax.ShapeDtyp...  6.29 us

commit v1 on v0

v1 whole, which is shorter than its diff:
```python
import functools

import jax
import jax.numpy as jnp
from jax import lax
from jax.experimental import pallas as pl
from jax.experimental.pallas import tpu as pltpu
from jax.sharding import PartitionSpec as P

F32, BF16 = jnp.float32, jnp.bfloat16
SLAB = 8
NT = (((1,), (1,)), ((), ()))
TN = (((0,), (0,)), ((), ()))
NN = (((1,), (0,)), ((), ()))


def dot(a, b, dims):
    return lax.dot_general(a, b, dims, preferred_element_type=F32)


def exchange(
    n,
    chips,
    chunks,
    cot_ref,
    in_ref,
    pre_ref,
    wu_ref,
    wd_ref,
    cot_out,
    in_out,
    act_out,
    gp_out,
    gi_out,
    cot_v,
    in_v,
    pre_v,
    wu_v,
    wd_v,
    cot_g,
    in_g,
    spread,
    cot_2,
    cot_f,
    active_f,
    gp_f,
    own,
    p1_s,
    p1_r,
    p2_s,
    p2_r,
    gp_2,
    rs_s,
    rs_r,
    local,
    cs,
    cr,
    is_,
    ir,
    s1,
    r1,
    s2,
    r2,
    s3,
    r3,
    s4,
    r4,
):
    me = lax.axis_index("fs")
    tp = lax.axis_index("tp")
    core = lax.rem(tp, 2)
    rows = cot_v.shape[0]
    width = wd_v.shape[1]
    half = n // 2
    group = half * rows
    side, place_in = me // half, lax.rem(me, half)
    sides = (side, 1 - side)
    first_row = [pl.multiple_of(g * group, 8) for g in sides]
    near = [half * side + lax.rem(place_in + k, half) for k in range(1, half)]
    far = [half * (1 - side) + q for q in range(half)]
    partner = tp + 1 - 2 * core
    x_peer = [None] + [lax.rem(tp + 2 * k, 2 * chips) for k in range(1, chips)]

    barrier = pltpu.get_barrier_semaphore()
    for p in far + near:
        pl.semaphore_signal(barrier, inc=1, device_id={"fs": p})
    pl.semaphore_signal(barrier, inc=1, device_id={"tp": partner})

    @pl.when(core == 1)
    def _():
        for k in range(1, chips):
            pl.semaphore_signal(barrier, inc=1, device_id={"tp": x_peer[k]})

    load_cot = pltpu.make_async_copy(cot_ref, cot_v, local.at[0])
    load_in = pltpu.make_async_copy(in_ref, in_v, local.at[1])
    load_cot.start()
    load_in.start()
    load_wd, load_pre, load_wu = [], [], []
    for j in range(chunks):
        load_wd.append(
            pltpu.make_async_copy(
                wd_ref.at[pl.ds(j * width, width)], wd_v.at[j], local.at[4 + j]
            )
        )
        load_wd[-1].start()
    for j in range(chunks):
        load_pre.append(
            pltpu.make_async_copy(
                pre_ref.at[:, pl.ds(j * width, width)],
                pre_v.at[j],
                local.at[4 + chunks + j],
            )
        )
        load_pre[-1].start()
    for j in range(chunks):
        load_wu.append(
            pltpu.make_async_copy(
                wu_ref.at[:, pl.ds(j * width, width)],
                wu_v.at[j],
                local.at[4 + 2 * chunks + j],
            )
        )
        load_wu[-1].start()
    spread[...] = jnp.zeros_like(spread)
    load_cot.wait()
    load_in.wait()
    own_cot = pltpu.make_async_copy(cot_v, cot_g.at[me], local.at[2])
    own_in = pltpu.make_async_copy(in_v, in_g.at[me], local.at[3])
    own_cot.start()
    own_in.start()

    def to_fs(src, dst, send_sem, recv_sem, p):
        return pltpu.make_async_remote_copy(
            src, dst.at[me], send_sem.at[p], recv_sem.at[me], device_id={"fs": p}
        )

    def from_fs(src, dst, send_sem, recv_sem, p):
        return pltpu.make_async_remote_copy(
            src, dst.at[p], send_sem.at[p], recv_sem.at[p], device_id={"fs": p}
        )

    pl.semaphore_wait(barrier, n + core * (chips - 1))
    for p in far[::-1] + near:
        to_fs(cot_v, cot_g, cs, cr, p).start()

    def picker(shape, token_dim):
        t = lax.broadcasted_iota(jnp.int32, shape, token_dim)
        j = lax.broadcasted_iota(jnp.int32, shape, 1 - token_dim)
        q, r = j // SLAB, j % SLAB
        return ((t == q * rows + r) & (r < rows)).astype(F32).astype(BF16)

    pick = picker((group, half * SLAB), 0)
    place = picker((half * SLAB, group), 1)

    def gathered(ref, g):
        for s in range(half):
            spread[s * SLAB : s * SLAB + rows, :] = ref[half * g + s].astype(F32)
        return dot(pick, spread[...].astype(BF16), NN)

    def gather_cot(ph):
        for p in (near, far)[ph]:
            from_fs(cot_v, cot_g, cs, cr, p).wait_recv()
        block = gathered(cot_g, sides[ph])
        cot_f[pl.ds(first_row[ph], group), :] = block
        cot_2[ph] = block.astype(BF16)

    def between(src, dst, send_sem, recv_sem, ph, j, to):
        return pltpu.make_async_remote_copy(
            src.at[ph, j],
            dst.at[ph, j],
            send_sem.at[ph, j],
            recv_sem.at[ph, j],
            device_id={"tp": to},
        )

    def to_chip(ph, j, k):
        return pltpu.make_async_remote_copy(
            p2_s.at[ph, j],
            p2_r.at[k - 1, ph, j],
            s2.at[k - 1, ph, j],
            r2.at[k - 1, ph, j],
            device_id={"tp": x_peer[k]},
        )

    def first_sum(ph, j):
        return between(p1_s, p1_r, s1, r1, ph, j, partner)

    def share(ph, j):
        return between(gp_2, gp_2, s3, r3, ph, j, partner)

    def lower(ph):
        for j in range(chunks):
            p1_s[ph, j] = dot(cot_2[ph], wd_v[j], NT).astype(BF16)
            first_sum(ph, j).start()

    def join(ph, j):
        first_sum(ph, j).wait_recv()
        total = own[ph, j] + p1_r[ph, j].astype(F32)
        own[ph, j] = total
        p2_s[ph, j] = total.astype(BF16)
        for k in range(1, chips):
            to_chip(ph, j, k).start()

    def upper(ph):
        own[ph, 0] = dot(cot_2[ph], wd_v[0], NT)
        for j in range(1, chunks):
            own[ph, j] = dot(cot_2[ph], wd_v[j], NT)
            join(ph, j - 1)
        join(ph, chunks - 1)

    def keep(ph, j):
        gp_f[j, pl.ds(first_row[ph], group), :] = gp_2[ph, j].astype(F32)

    def finish(ph, j):
        hidden = own[ph, j]
        for k in range(1, chips):
            to_chip(ph, j, k).wait_recv()
            hidden = hidden + p2_r[k - 1, ph, j].astype(F32)
        active = active_f[j, pl.ds(first_row[ph], group), :]
        gp_2[ph, j] = (2.0 * active * hidden).astype(BF16)
        share(ph, j).start()

    def accumulate_lower(ph):
        acc = None
        for j in range(chunks):
            share(ph, j).wait_recv()
            term = dot(gp_2[ph, j], wu_v[j], NT)
            acc = term if acc is None else acc + term
        return acc

    def accumulate_upper(ph):
        acc = None
        for j in range(chunks):
            finish(ph, j)
            term = dot(gp_2[ph, j], wu_v[j], NT)
            acc = term if acc is None else acc + term
        return acc

    def scatter_copies(ph):
        if ph == 0:
            return [
                pltpu.make_async_remote_copy(
                    rs_s.at[0, lax.rem(place_in + k, half)],
                    rs_r.at[k],
                    s4.at[k],
                    r4.at[k],
                    device_id={"fs": near[k - 1]},
                )
                for k in range(1, half)
            ]
        return [
            pltpu.make_async_remote_copy(
                rs_s.at[1, q],
                rs_r.at[half + place_in],
                s4.at[half + q],
                r4.at[half + place_in],
                device_id={"fs": far[q]},
            )
            for q in range(half)
        ]

    def scatter(ph, acc):
        slabs = dot(place, acc.astype(BF16), NN)
        for s in range(half):
            rs_s[ph, s] = slabs[s * SLAB : s * SLAB + rows, :].astype(BF16)
        for copy in scatter_copies(ph):
            copy.start()

    def share_inputs():
        for p in far + near:
            to_fs(in_v, in_g, is_, ir, p).start()

    def activate():
        for copy in load_pre:
            copy.wait()
        for j in range(chunks):
            active = jnp.maximum(pre_v[j].astype(F32), 0.0)
            active_f[j] = active
            act_out[j] = (active * active).astype(BF16)

    for copy in load_wd:
        copy.wait()
    own_cot.wait()
    gather_cot(0)

    @pl.when(core == 0)
    def _():
        lower(0)
        gather_cot(1)
        lower(1)
        share_inputs()
        activate()
        for copy in load_wu:
            copy.wait()
        scatter(0, accumulate_lower(0))
        scatter(1, accumulate_lower(1))

    @pl.when(core == 1)
    def _():
        upper(0)
        gather_cot(1)
        upper(1)
        share_inputs()
        activate()
        for copy in load_wu:
            copy.wait()
        scatter(0, accumulate_upper(0))
        scatter(1, accumulate_upper(1))

    cot_out[...] = cot_f[...].astype(BF16)
    for ph in range(2):
        for j in range(chunks):
            keep(ph, j)
    gp_out[...] = gp_f[...].astype(BF16)
    own_in.wait()
    for p in near + far:
        from_fs(in_v, in_g, is_, ir, p).wait_recv()
    for g in range(2):
        cot_f[g * group : (g + 1) * group, :] = gathered(in_g, g)
    in_out[...] = cot_f[...].astype(BF16)

    for p in far + near:
        to_fs(cot_v, cot_g, cs, cr, p).wait_send()
        to_fs(in_v, in_g, is_, ir, p).wait_send()

    @pl.when(core == 0)
    def _():
        for ph in range(2):
            for j in range(chunks):
                first_sum(ph, j).wait_send()

    @pl.when(core == 1)
    def _():
        for ph in range(2):
            for j in range(chunks):
                for k in range(1, chips):
                    to_chip(ph, j, k).wait_send()
                share(ph, j).wait_send()

    total = rs_s[0, place_in].astype(F32)
    for copy, k in zip(scatter_copies(0), range(1, half)):
        copy.wait_recv()
        total = total + rs_r[k].astype(F32)
    for q in range(half):
        pltpu.make_async_remote_copy(
            rs_s.at[1, q],
            rs_r.at[half + q],
            s4.at[half + q],
            r4.at[half + q],
            device_id={"fs": far[q]},
        ).wait_recv()
        total = total + rs_r[half + q].astype(F32)
    gi_out[...] = total.astype(BF16)
    for ph in range(2):
        for copy in scatter_copies(ph):
            copy.wait_send()


def outer(
    chunks, cot_v, in_v, act_v, gp_v, gi_v, gi_out, gu_out, gd_out, gu_v, gd_v, sem
):
    width = gp_v.shape[2]
    pieces = []

    def put(src, dst):
        copy = pltpu.make_async_copy(src, dst, sem.at[len(pieces)])
        copy.start()
        pieces.append(copy)

    half = width // 2
    for j in range(chunks):
        for h in range(2):
            rows = pl.ds(j * width + h * half, half)
            gd_v[rows, :] = dot(act_v[j, :, h * half : (h + 1) * half], cot_v[...], TN)
            put(gd_v.at[rows], gd_out.at[rows])
    put(gi_v, gi_out)
    step = in_v.shape[1] // (2 * chunks)
    for i in range(2 * chunks):
        rows = pl.ds(i * step, step)
        for j in range(chunks):
            gu_v[rows, j * width : (j + 1) * width] = dot(
                in_v[:, i * step : (i + 1) * step], gp_v[j], TN
            )
        put(gu_v.at[rows], gu_out.at[rows])
    for copy in pieces:
        copy.wait()


def fused(n, ntp, inputs, cotangent, pre_act, w_up, w_down):
    rows, d = inputs.shape
    tokens, ff = pre_act.shape
    chips = ntp // 2
    half = n // 2
    group = half * rows
    chunks = 4 if ff % 1024 == 0 else 2
    width = ff // chunks
    hbm = pl.BlockSpec(memory_space=pl.ANY)
    vmem = pl.BlockSpec(memory_space=pltpu.VMEM)
    dma = pltpu.SemaphoreType.DMA
    cot, full, act, gp, gi = pl.pallas_call(
        functools.partial(exchange, n, chips, chunks),
        out_shape=(
            pltpu.VMEM((tokens, d), BF16),
            pltpu.VMEM((tokens, d), BF16),
            pltpu.VMEM((chunks, tokens, width), BF16),
            pltpu.VMEM((chunks, tokens, width), BF16),
            pltpu.VMEM((rows, d), BF16),
        ),
        in_specs=[hbm] * 5,
        out_specs=(vmem,) * 5,
        scratch_shapes=[
            pltpu.VMEM((rows, d), BF16),
            pltpu.VMEM((rows, d), BF16),
            pltpu.VMEM((chunks, tokens, width), BF16),
            pltpu.VMEM((chunks, d, width), BF16),
            pltpu.VMEM((chunks, width, d), BF16),
            pltpu.VMEM((n, rows, d), BF16),
            pltpu.VMEM((n, rows, d), BF16),
            pltpu.VMEM((half * SLAB, d), F32),
            pltpu.VMEM((2, group, d), BF16),
            pltpu.VMEM((tokens, d), F32),
            pltpu.VMEM((chunks, tokens, width), F32),
            pltpu.VMEM((chunks, tokens, width), F32),
            pltpu.VMEM((2, chunks, group, width), F32),
            pltpu.VMEM((2, chunks, group, width), BF16),
            pltpu.VMEM((2, chunks, group, width), BF16),
            pltpu.VMEM((2, chunks, group, width), BF16),
            pltpu.VMEM((chips - 1, 2, chunks, group, width), BF16),
            pltpu.VMEM((2, chunks, group, width), BF16),
            pltpu.VMEM((2, half, rows, d), BF16),
            pltpu.VMEM((n, rows, d), BF16),
            dma((4 + 3 * chunks,)),
            dma((n,)),
            dma((n,)),
            dma((n,)),
            dma((n,)),
            dma((2, chunks)),
            dma((2, chunks)),
            dma((chips - 1, 2, chunks)),
            dma((chips - 1, 2, chunks)),
            dma((2, chunks)),
            dma((2, chunks)),
            dma((n,)),
            dma((n,)),
        ],
        compiler_params=pltpu.CompilerParams(collective_id=0, has_side_effects=True),
    )(cotangent, inputs, pre_act, w_up, w_down)
    return pl.pallas_call(
        functools.partial(outer, chunks),
        out_shape=(
            jax.ShapeDtypeStruct((rows, d), BF16),
            jax.ShapeDtypeStruct((d, ff), F32),
            jax.ShapeDtypeStruct((ff, d), F32),
        ),
        in_specs=[vmem] * 5,
        out_specs=(hbm,) * 3,
        scratch_shapes=[
            pltpu.VMEM((d, ff), F32),
            pltpu.VMEM((ff, d), F32),
            dma((4 * chunks + 1,)),
        ],
    )(*(pltpu.with_memory_space_constraint(x, pltpu.VMEM) for x in (cot, full, act, gp, gi)))


def plain(inputs, cotangent, pre_act, w_up, w_down):
    active = jax.nn.relu(pre_act.astype(F32))
    squared = jnp.square(active).astype(BF16)
    piece = lax.all_gather(cotangent, "fs", axis=0, tiled=True)
    grad_down = dot(squared, piece, TN)
    hidden = lax.psum(dot(piece, w_down, NT).astype(BF16), "tp").astype(F32)
    grad_pre = (2.0 * active * hidden).astype(BF16)
    grad_up = dot(lax.all_gather(inputs, "fs", axis=0, tiled=True), grad_pre, TN)
    grad_input = lax.psum_scatter(
        dot(grad_pre, w_up, NT), "fs", scatter_dimension=0, tiled=True
    ).astype(BF16)
    return (grad_input, grad_up, grad_down)


def solution(mesh):
    n, ntp = mesh.shape["fs"], mesh.shape["tp"]

    def body(inputs, cotangent, pre_act, w_up, w_down):
        rows, d = inputs.shape
        tokens, ff = pre_act.shape
        if (
            n == 8
            and ntp > 2
            and ntp % 2 == 0
            and rows <= SLAB
            and tokens % 16 == 0
            and d % 1024 == 0
            and ff % 1024 == 0
        ):
            return fused(n, ntp, inputs, cotangent, pre_act, w_up, w_down)
        return plain(inputs, cotangent, pre_act, w_up, w_down)

    return jax.shard_map(
        body,
        mesh=mesh,
        in_specs=(P("fs", "tp"), P("fs", "tp"), P(None, "fs"), P("tp", "fs"), P("fs", "tp")),
        out_specs=(P("fs", "tp"), P("tp", "fs"), P("fs", "tp")),
        check_vma=False,
    )
```

time: 31.1 us -> 30.6 us (0.984)
  Pallas kernels: 30.2 us -> 29.7 us
    pallas_call x1, Pallas kernels: 23.9 us -> 23.4 us  [fused(): pl.pallas_call(functools.partial(exchange, n, chips, chunks), out_shape=(...]
where the time goes in v1:
time: 30.6 us; the launch traced here: 30.4 us
  Pallas kernels  29.7 us (97%)
  between operations  0.64 us (2%)
    pallas_call x1, Pallas kernels, fused(): pl.pallas_call(functools.partial(exchange, n, chips, chunks), out_shape=(...  23.4 us
    pallas_call x1, Pallas kernels, fused(): pl.pallas_call(functools.partial(outer, chunks), out_shape=(jax.ShapeDtyp...  6.29 us

profile of v1, /device:TPU:0, one launch (start us, length us, event | category | flops | bytes accessed | tf_op | source)
XLA Modules:
  0.0 30.4 jit_solution(1385042779612494218)
XLA Ops:
  0.6 23.4 %shard_map.76 = (bf16[48,1024]{1,0:T(8,128)(2,1)S(1)}, bf16[48,1024]{1,0:T(8,128)(2,1)S(1)}, bf16[4,48,512]{2,1,0:T(8,128)(2,1)S(1)}, bf16[4,48,512]{2,1,0:T(8,128)(2,1)S(1)}, bf16[6,1024]{1,0:T(8,128)(2,1)S(1)}) custom-call(bf16[6,1024]{1,0:T(8,128)(2,1)} %cot_ref.1, bf16[6,1024]{1,0:T(8,128)(2,1)} %in_ref.1, bf16[48,2048]{1,0:T(8,128)(2,1)} %pre_ref.1, ...), custom_call_target="tpu_custom_call" | custom-call | tf_op jit(solution)/shard_map/pallas_call | solution.py:400
  24.1 6.3 %shard_map.77 = (bf16[6,1024]{1,0:T(8,128)(2,1)}, f32[1024,2048]{1,0:T(8,128)}, f32[2048,1024]{1,0:T(8,128)}) custom-call(bf16[48,1024]{1,0:T(8,128)(2,1)S(1)} %get-tuple-element.8.cot_v, bf16[48,1024]{1,0:T(8,128)(2,1)S(1)} %get-tuple-element.9.in_v, bf16[4,48,512]{2,1,0:T(8,128)(2,1)S(1)} %get-tuple-element.10.act_v, ...), custom_call_target="tpu_custom_call" | custom-call | tf_op jit(solution)/shard_map/pallas_call | solution.py:448

commit v2 on v1

v2 whole, which is shorter than its diff:
```python
import functools

import jax
import jax.numpy as jnp
from jax import lax
from jax.experimental import pallas as pl
from jax.experimental.pallas import tpu as pltpu
from jax.sharding import PartitionSpec as P

F32, BF16 = jnp.float32, jnp.bfloat16
SLAB = 8
CHUNKS = 4
RAW = 4
NT = (((1,), (1,)), ((), ()))
TN = (((0,), (0,)), ((), ()))
NN = (((1,), (0,)), ((), ()))


def dot(a, b, dims):
    return lax.dot_general(a, b, dims, preferred_element_type=F32)


def exchange(
    n,
    chips,
    chunks,
    direct,
    cot_ref,
    in_ref,
    pre_ref,
    wu_ref,
    wd_ref,
    cot_out,
    in_out,
    act_out,
    gp_out,
    gi_out,
    cot_v,
    in_v,
    pre_v,
    wu_v,
    wd_v,
    cot_g,
    in_g,
    spread,
    own,
    p1_s,
    p1_r,
    p2_s,
    p2_r,
    raw_r,
    rs_s,
    rs_r,
    local,
    cs,
    cr,
    is_,
    ir,
    s1,
    r1,
    s2,
    r2,
    s3,
    r3,
    s4,
    r4,
    s5,
    r5,
    ready,
):
    me = lax.axis_index("fs")
    tp = lax.axis_index("tp")
    core = lax.rem(tp, 2)
    rows = cot_v.shape[0]
    width = wd_v.shape[1]
    tokens = n * rows
    half = n // 2
    side, spot = me // half, lax.rem(me, half)
    near = [half * side + lax.rem(spot + k, half) for k in range(1, half)]
    far = [half * (1 - side) + q for q in range(half)]
    partner = tp + 1 - 2 * core
    x_peer = [None] + [lax.rem(tp + 1 - core + 2 * k, 2 * chips) for k in range(1, chips)]

    barrier = pltpu.get_barrier_semaphore()
    for p in far + near:
        pl.semaphore_signal(barrier, inc=1, device_id={"fs": p})
    pl.semaphore_signal(barrier, inc=1, device_id={"tp": partner})

    @pl.when(core == 1)
    def _():
        for k in range(1, chips):
            pl.semaphore_signal(barrier, inc=1, device_id={"tp": x_peer[k]})

    load_cot = pltpu.make_async_copy(cot_ref, cot_v, local.at[0])
    load_in = pltpu.make_async_copy(in_ref, in_v, local.at[1])
    load_cot.start()
    load_in.start()
    load_wd, load_pre, load_wu = [], [], []
    for j in range(chunks):
        load_wd.append(
            pltpu.make_async_copy(
                wd_ref.at[pl.ds(j * width, width)], wd_v.at[j], local.at[4 + j]
            )
        )
        load_wd[-1].start()
    for j in range(chunks):
        load_pre.append(
            pltpu.make_async_copy(
                pre_ref.at[:, pl.ds(j * width, width)],
                pre_v.at[j],
                local.at[4 + chunks + j],
            )
        )
        load_pre[-1].start()
    for j in range(chunks):
        load_wu.append(
            pltpu.make_async_copy(
                wu_ref.at[:, pl.ds(j * width, width)],
                wu_v.at[j],
                local.at[4 + 2 * chunks + j],
            )
        )
        load_wu[-1].start()
    spread[...] = jnp.zeros_like(spread)
    load_cot.wait()
    load_in.wait()
    own_cot = pltpu.make_async_copy(cot_v, cot_g.at[me], local.at[2])
    own_in = pltpu.make_async_copy(in_v, in_g.at[me], local.at[3])
    own_cot.start()
    own_in.start()

    def to_fs(src, dst, send_sem, recv_sem, p):
        return pltpu.make_async_remote_copy(
            src, dst.at[me], send_sem.at[p], recv_sem.at[me], device_id={"fs": p}
        )

    def from_fs(src, dst, send_sem, recv_sem, p):
        return pltpu.make_async_remote_copy(
            src, dst.at[p], send_sem.at[p], recv_sem.at[p], device_id={"fs": p}
        )

    pl.semaphore_wait(barrier, n + core * (chips - 1))

    @pl.when(core == 1)
    def _():
        pl.semaphore_signal(ready, inc=1, device_id={"tp": partner})

    for p in far[::-1] + near:
        to_fs(cot_v, cot_g, cs, cr, p).start()

    def picker(shape, token_dim):
        t = lax.broadcasted_iota(jnp.int32, shape, token_dim)
        j = lax.broadcasted_iota(jnp.int32, shape, 1 - token_dim)
        q, r = j // SLAB, j % SLAB
        return ((t == q * rows + r) & (r < rows)).astype(F32).astype(BF16)

    pick = picker((tokens, n * SLAB), 0)
    place = picker((n * SLAB, tokens), 1)

    def gathered(ref):
        for s in range(n):
            spread[s * SLAB : s * SLAB + rows, :] = ref[s].astype(F32)
        return spread[...].astype(BF16)

    def between(src, dst, send_sem, recv_sem, j):
        return pltpu.make_async_remote_copy(
            src.at[j], dst.at[j], send_sem.at[j], recv_sem.at[j], device_id={"tp": partner}
        )

    def to_chip(j, k):
        return pltpu.make_async_remote_copy(
            p2_s.at[j],
            p2_r.at[k - 1, j],
            s2.at[k - 1, j],
            r2.at[k - 1, j],
            device_id={"tp": x_peer[k]},
        )

    def direct_to_chip(j, k, src, c):
        return pltpu.make_async_remote_copy(
            src.at[j],
            raw_r.at[k - 1, c, j],
            s5.at[k - 1, j],
            r5.at[k - 1, c, j],
            device_id={"tp": x_peer[k]},
        )

    def first_sum(j):
        return between(p1_s, p1_r, s1, r1, j)

    def share(j):
        return between(gp_out, gp_out, s3, r3, j)

    def lower():
        for j in range(chunks):
            p1_s[j] = dot(cot_out[...], wd_v[j], NT).astype(BF16)
            first_sum(j).start()
            if j == 0:
                pl.semaphore_wait(ready, 1)
            if j < direct:
                for k in range(1, chips):
                    direct_to_chip(j, k, p1_s, 0).start()

    def join(j):
        first_sum(j).wait_recv()
        total = own[j] + p1_r[j].astype(F32)
        own[j] = total
        p2_s[j] = total.astype(BF16)
        for k in range(1, chips):
            to_chip(j, k).start()

    def upper():
        for j in range(chunks):
            own[j] = dot(cot_out[...], wd_v[j], NT)
            if j < direct:
                p2_s[j] = own[j].astype(BF16)
                for k in range(1, chips):
                    direct_to_chip(j, k, p2_s, 1).start()
        for j in range(direct, chunks):
            join(j)

    def finish(j):
        hidden = own[j]
        if j < direct:
            first_sum(j).wait_recv()
            hidden = hidden + p1_r[j].astype(F32)
        for k in range(1, chips):
            if j < direct:
                for c in (1, 0):
                    direct_to_chip(j, k, p2_s, c).wait_recv()
                    hidden = hidden + raw_r[k - 1, c, j].astype(F32)
            else:
                to_chip(j, k).wait_recv()
                hidden = hidden + p2_r[k - 1, j].astype(F32)
        active = jnp.maximum(pre_v[j].astype(F32), 0.0)
        gp = (2.0 * active * hidden).astype(BF16)
        gp_out[j] = dot(place, gp, NN).astype(BF16)
        share(j).start()

    def obtain(j):
        share(j).wait_recv()

    def accumulate(ready):
        acc = None
        for j in range(chunks):
            ready(j)
            term = dot(gp_out[j], wu_v[j], NT)
            acc = term if acc is None else acc + term
        for s in range(n):
            rs_s[s] = acc[s * SLAB : s * SLAB + rows, :].astype(BF16)
        for p in far + near:
            to_fs(rs_s.at[p], rs_r, s4, r4, p).start()

    def share_inputs():
        for p in far + near:
            to_fs(in_v, in_g, is_, ir, p).start()

    def activate():
        for copy in load_pre:
            copy.wait()
        for j in range(chunks):
            active = jnp.maximum(pre_v[j].astype(F32), 0.0)
            act_out[j] = (active * active).astype(BF16)

    for copy in load_wd:
        copy.wait()
    own_cot.wait()
    for p in near + far:
        from_fs(cot_v, cot_g, cs, cr, p).wait_recv()
    cot_out[...] = dot(pick, gathered(cot_g), NN).astype(BF16)

    @pl.when(core == 0)
    def _():
        lower()
        share_inputs()
        activate()
        for copy in load_wu:
            copy.wait()
        accumulate(obtain)

    @pl.when(core == 1)
    def _():
        upper()
        share_inputs()
        activate()
        for copy in load_wu:
            copy.wait()
        accumulate(finish)

    own_in.wait()
    for p in near + far:
        from_fs(in_v, in_g, is_, ir, p).wait_recv()
    in_out[...] = gathered(in_g)

    for p in far + near:
        to_fs(cot_v, cot_g, cs, cr, p).wait_send()
        to_fs(in_v, in_g, is_, ir, p).wait_send()

    @pl.when(core == 0)
    def _():
        for j in range(chunks):
            first_sum(j).wait_send()
            if j < direct:
                for k in range(1, chips):
                    direct_to_chip(j, k, p1_s, 0).wait_send()

    @pl.when(core == 1)
    def _():
        for j in range(chunks):
            for k in range(1, chips):
                if j < direct:
                    direct_to_chip(j, k, p2_s, 1).wait_send()
                else:
                    to_chip(j, k).wait_send()
            share(j).wait_send()

    total = rs_s[me].astype(F32)
    for p in near + far:
        from_fs(rs_s.at[p], rs_r, s4, r4, p).wait_recv()
        total = total + rs_r[p].astype(F32)
    gi_out[...] = total.astype(BF16)
    for p in far + near:
        to_fs(rs_s.at[p], rs_r, s4, r4, p).wait_send()


def outer(
    chunks, cot_v, in_v, act_v, gp_v, gi_v, gi_out, gu_out, gd_out, gu_v, gd_v, sem
):
    width = gp_v.shape[2]
    pieces = []

    def put(src, dst):
        copy = pltpu.make_async_copy(src, dst, sem.at[len(pieces)])
        copy.start()
        pieces.append(copy)

    half = width // 2
    for j in range(chunks):
        for h in range(2):
            rows = pl.ds(j * width + h * half, half)
            gd_v[rows, :] = dot(act_v[j, :, h * half : (h + 1) * half], cot_v[...], TN)
            put(gd_v.at[rows], gd_out.at[rows])
    put(gi_v, gi_out)
    step = in_v.shape[1] // (2 * chunks)
    for i in range(2 * chunks):
        rows = pl.ds(i * step, step)
        for j in range(chunks):
            gu_v[rows, j * width : (j + 1) * width] = dot(
                in_v[:, i * step : (i + 1) * step], gp_v[j], TN
            )
        put(gu_v.at[rows], gu_out.at[rows])
    for copy in pieces:
        copy.wait()


def fused(n, ntp, inputs, cotangent, pre_act, w_up, w_down):
    rows, d = inputs.shape
    tokens, ff = pre_act.shape
    chips = ntp // 2
    chunks = CHUNKS
    width = ff // chunks
    hbm = pl.BlockSpec(memory_space=pl.ANY)
    vmem = pl.BlockSpec(memory_space=pltpu.VMEM)
    dma = pltpu.SemaphoreType.DMA
    cot, full, act, gp, gi = pl.pallas_call(
        functools.partial(exchange, n, chips, chunks, RAW),
        out_shape=(
            pltpu.VMEM((tokens, d), BF16),
            pltpu.VMEM((n * SLAB, d), BF16),
            pltpu.VMEM((chunks, tokens, width), BF16),
            pltpu.VMEM((chunks, n * SLAB, width), BF16),
            pltpu.VMEM((rows, d), BF16),
        ),
        in_specs=[hbm] * 5,
        out_specs=(vmem,) * 5,
        scratch_shapes=[
            pltpu.VMEM((rows, d), BF16),
            pltpu.VMEM((rows, d), BF16),
            pltpu.VMEM((chunks, tokens, width), BF16),
            pltpu.VMEM((chunks, d, width), BF16),
            pltpu.VMEM((chunks, width, d), BF16),
            pltpu.VMEM((n, rows, d), BF16),
            pltpu.VMEM((n, rows, d), BF16),
            pltpu.VMEM((n * SLAB, d), F32),
            pltpu.VMEM((chunks, tokens, width), F32),
            pltpu.VMEM((chunks, tokens, width), BF16),
            pltpu.VMEM((chunks, tokens, width), BF16),
            pltpu.VMEM((chunks, tokens, width), BF16),
            pltpu.VMEM((chips - 1, chunks, tokens, width), BF16),
            pltpu.VMEM((chips - 1, 2, RAW, tokens, width), BF16),
            pltpu.VMEM((n, rows, d), BF16),
            pltpu.VMEM((n, rows, d), BF16),
            dma((4 + 3 * chunks,)),
            dma((n,)),
            dma((n,)),
            dma((n,)),
            dma((n,)),
            dma((chunks,)),
            dma((chunks,)),
            dma((chips - 1, chunks)),
            dma((chips - 1, chunks)),
            dma((chunks,)),
            dma((chunks,)),
            dma((n,)),
            dma((n,)),
            dma((chips - 1, RAW)),
            dma((chips - 1, 2, RAW)),
            pltpu.SemaphoreType.REGULAR,
        ],
        compiler_params=pltpu.CompilerParams(collective_id=0, has_side_effects=True),
    )(cotangent, inputs, pre_act, w_up, w_down)
    return pl.pallas_call(
        functools.partial(outer, chunks),
        out_shape=(
            jax.ShapeDtypeStruct((rows, d), BF16),
            jax.ShapeDtypeStruct((d, ff), F32),
            jax.ShapeDtypeStruct((ff, d), F32),
        ),
        in_specs=[vmem] * 5,
        out_specs=(hbm,) * 3,
        scratch_shapes=[
            pltpu.VMEM((d, ff), F32),
            pltpu.VMEM((ff, d), F32),
            dma((4 * chunks + 1,)),
        ],
    )(*(pltpu.with_memory_space_constraint(x, pltpu.VMEM) for x in (cot, full, act, gp, gi)))


def plain(inputs, cotangent, pre_act, w_up, w_down):
    active = jax.nn.relu(pre_act.astype(F32))
    squared = jnp.square(active).astype(BF16)
    piece = lax.all_gather(cotangent, "fs", axis=0, tiled=True)
    grad_down = dot(squared, piece, TN)
    hidden = lax.psum(dot(piece, w_down, NT).astype(BF16), "tp").astype(F32)
    grad_pre = (2.0 * active * hidden).astype(BF16)
    grad_up = dot(lax.all_gather(inputs, "fs", axis=0, tiled=True), grad_pre, TN)
    grad_input = lax.psum_scatter(
        dot(grad_pre, w_up, NT), "fs", scatter_dimension=0, tiled=True
    ).astype(BF16)
    return (grad_input, grad_up, grad_down)


def solution(mesh):
    n, ntp = mesh.shape["fs"], mesh.shape["tp"]

    def body(inputs, cotangent, pre_act, w_up, w_down):
        rows, d = inputs.shape
        tokens, ff = pre_act.shape
        if (
            n == 8
            and ntp > 2
            and ntp % 2 == 0
            and rows <= SLAB
            and tokens % 16 == 0
            and d % 1024 == 0
            and ff % 1024 == 0
        ):
            return fused(n, ntp, inputs, cotangent, pre_act, w_up, w_down)
        return plain(inputs, cotangent, pre_act, w_up, w_down)

    return jax.shard_map(
        body,
        mesh=mesh,
        in_specs=(P("fs", "tp"), P("fs", "tp"), P(None, "fs"), P("tp", "fs"), P("fs", "tp")),
        out_specs=(P("fs", "tp"), P("tp", "fs"), P("fs", "tp")),
        check_vma=False,
    )
```

time: 30.6 us -> 29.7 us (0.971)
  Pallas kernels: 29.7 us -> 28.8 us
    pallas_call x1, Pallas kernels: 23.4 us -> 22.5 us  [fused(): pl.pallas_call(functools.partial(exchange, n, chips, chunks, RAW), out_sh...]
where the time goes in v2:
time: 29.7 us; the launch traced here: 29.5 us
  Pallas kernels  28.8 us (97%)
  between operations  0.64 us (2%)
    pallas_call x1, Pallas kernels, fused(): pl.pallas_call(functools.partial(exchange, n, chips, chunks, RAW), out_sh...  22.5 us
    pallas_call x1, Pallas kernels, fused(): pl.pallas_call(functools.partial(outer, chunks), out_shape=(jax.ShapeDtyp...  6.29 us

profile of v2, /device:TPU:0, one launch (start us, length us, event | category | flops | bytes accessed | tf_op | source)
XLA Modules:
  0.0 29.5 jit_solution(12550951285408894718)
XLA Ops:
  0.6 22.5 %shard_map.76 = (bf16[48,1024]{1,0:T(8,128)(2,1)S(1)}, bf16[64,1024]{1,0:T(8,128)(2,1)S(1)}, bf16[4,48,512]{2,1,0:T(8,128)(2,1)S(1)}, bf16[4,64,512]{2,1,0:T(8,128)(2,1)S(1)}, bf16[6,1024]{1,0:T(8,128)(2,1)S(1)}) custom-call(bf16[6,1024]{1,0:T(8,128)(2,1)} %cot_ref.1, bf16[6,1024]{1,0:T(8,128)(2,1)} %in_ref.1, bf16[48,2048]{1,0:T(8,128)(2,1)} %pre_ref.1, ...), custom_call_target="tpu_custom_call" | custom-call | tf_op jit(solution)/shard_map/pallas_call | solution.py:365
  23.2 6.3 %shard_map.77 = (bf16[6,1024]{1,0:T(8,128)(2,1)}, f32[1024,2048]{1,0:T(8,128)}, f32[2048,1024]{1,0:T(8,128)}) custom-call(bf16[48,1024]{1,0:T(8,128)(2,1)S(1)} %get-tuple-element.8.cot_v, bf16[64,1024]{1,0:T(8,128)(2,1)S(1)} %get-tuple-element.9.in_v, bf16[4,48,512]{2,1,0:T(8,128)(2,1)S(1)} %get-tuple-element.10.act_v, ...), custom_call_target="tpu_custom_call" | custom-call | tf_op jit(solution)/shard_map/pallas_call | solution.py:412

commit v3 on v2

v3 whole, which is shorter than its diff:
```python
import functools

import jax
import jax.numpy as jnp
from jax import lax
from jax.experimental import pallas as pl
from jax.experimental.pallas import tpu as pltpu
from jax.sharding import PartitionSpec as P

F32, BF16 = jnp.float32, jnp.bfloat16
SLAB = 8
CHUNKS = 4
AHEAD = 0
NT = (((1,), (1,)), ((), ()))
TN = (((0,), (0,)), ((), ()))
NN = (((1,), (0,)), ((), ()))


def dot(a, b, dims):
    return lax.dot_general(a, b, dims, preferred_element_type=F32)


def exchange(
    n,
    chips,
    chunks,
    cot_ref,
    in_ref,
    pre_ref,
    wu_ref,
    wd_ref,
    cot_out,
    in_out,
    act_out,
    gp_out,
    gi_out,
    own_v,
    pre_v,
    wu_v,
    wd_v,
    land,
    spread,
    own,
    p1_s,
    p1_r,
    p2_s,
    p2_r,
    rs_s,
    local,
    fs_s,
    fs_r,
    tp_s,
    gp_s,
    tp_r,
    x_r,
):
    me = lax.axis_index("fs")
    tp = lax.axis_index("tp")
    core = lax.rem(tp, 2)
    cot_v, in_v = own_v.at[0], own_v.at[1]
    cot_g, in_g, rs_r = land.at[0], land.at[1], land.at[2]
    rows = own_v.shape[1]
    width = wd_v.shape[1]
    tokens = n * rows
    half = n // 2
    side, spot = me // half, lax.rem(me, half)
    near = [half * side + lax.rem(spot + k, half) for k in range(1, half)]
    far = [half * (1 - side) + q for q in range(half)]
    partner = tp + 1 - 2 * core
    x_peer = [None] + [lax.rem(tp - core + 2 * k, 2 * chips) for k in range(1, chips)]

    barrier = pltpu.get_barrier_semaphore()
    for p in far + near:
        pl.semaphore_signal(barrier, inc=1, device_id={"fs": p})
    pl.semaphore_signal(barrier, inc=1, device_id={"tp": partner})

    @pl.when(core == 0)
    def _():
        for k in range(1, chips):
            pl.semaphore_signal(barrier, inc=1, device_id={"tp": x_peer[k]})

    def settle(ref, sem):
        pltpu.make_async_copy(ref, ref, sem).wait()

    pltpu.make_async_copy(cot_ref, cot_v, local.at[0]).start()
    pltpu.make_async_copy(in_ref, in_v, local.at[0]).start()
    for j in range(chunks):
        pltpu.make_async_copy(
            wd_ref.at[pl.ds(j * width, width)], wd_v.at[j], local.at[1]
        ).start()
    for j in range(chunks):
        pltpu.make_async_copy(
            pre_ref.at[:, pl.ds(j * width, width)], pre_v.at[j], local.at[2]
        ).start()
    for j in range(chunks):
        pltpu.make_async_copy(
            wu_ref.at[:, pl.ds(j * width, width)], wu_v.at[j], local.at[3]
        ).start()
    spread[...] = jnp.zeros_like(spread)
    settle(own_v, local.at[0])
    land[0, me] = own_v[0]
    land[1, me] = own_v[1]

    def to_fs(src, kind, p):
        return pltpu.make_async_remote_copy(
            src, land.at[kind, me], fs_s, fs_r.at[kind], device_id={"fs": p}
        )

    def from_fs(kind):
        settle(land.at[kind, pl.ds(0, n - 1)], fs_r.at[kind])

    pl.semaphore_wait(barrier, n + (1 - core) * (chips - 1))
    for p in far[::-1] + near:
        to_fs(cot_v, 0, p).start()

    def picker(shape, token_dim):
        t = lax.broadcasted_iota(jnp.int32, shape, token_dim)
        j = lax.broadcasted_iota(jnp.int32, shape, 1 - token_dim)
        q, r = j // SLAB, j % SLAB
        return ((t == q * rows + r) & (r < rows)).astype(F32).astype(BF16)

    pick = picker((tokens, n * SLAB), 0)
    place = picker((n * SLAB, tokens), 1)

    def gathered(ref):
        for s in range(n):
            spread[s * SLAB : s * SLAB + rows, :] = ref[s].astype(F32)
        return spread[...].astype(BF16)

    def between(src, dst, send_sem, recv_sem, j):
        return pltpu.make_async_remote_copy(
            src.at[j], dst.at[j], send_sem, recv_sem.at[j], device_id={"tp": partner}
        )

    def to_chip(j, k):
        return pltpu.make_async_remote_copy(
            p2_s.at[j],
            p2_r.at[k - 1, j],
            tp_s,
            x_r.at[k - 1, j],
            device_id={"tp": x_peer[k]},
        )

    def first_sum(j):
        return between(p1_s, p1_r, tp_s, tp_r, j)

    def share(j):
        return between(gp_out, gp_out, gp_s, tp_r, j)

    def lower():
        for j in range(chunks):
            p1_s[j] = dot(cot_out[...], wd_v[j], NT).astype(BF16)
            first_sum(j).start()

    def join(j):
        first_sum(j).wait_recv()
        total = own[j] + p1_r[j].astype(F32)
        own[j] = total
        p2_s[j] = total.astype(BF16)
        for k in range(1, chips):
            to_chip(j, k).start()

    def upper():
        for j in range(chunks):
            own[j] = dot(cot_out[...], wd_v[j], NT)
            join(j)

    def finish(j):
        hidden = own[j]
        for k in range(1, chips):
            to_chip(j, k).wait_recv()
            hidden = hidden + p2_r[k - 1, j].astype(F32)
        active = jnp.maximum(pre_v[j].astype(F32), 0.0)
        gp = (2.0 * active * hidden).astype(BF16)
        gp_out[j] = dot(place, gp, NN).astype(BF16)
        share(j).start()

    def obtain(j):
        share(j).wait_recv()

    def accumulate(ready, ahead):
        acc = None
        for j in range(chunks + ahead):
            if j < chunks:
                ready(j)
            if j >= ahead:
                term = dot(gp_out[j - ahead], wu_v[j - ahead], NT)
                acc = term if acc is None else acc + term
        for s in range(n):
            rs_s[s] = acc[s * SLAB : s * SLAB + rows, :].astype(BF16)
        for p in far + near:
            to_fs(rs_s.at[p], 2, p).start()

    def share_inputs():
        for p in far + near:
            to_fs(in_v, 1, p).start()

    def activate():
        settle(pre_v, local.at[2])
        for j in range(chunks):
            active = jnp.maximum(pre_v[j].astype(F32), 0.0)
            act_out[j] = (active * active).astype(BF16)

    settle(wd_v, local.at[1])
    from_fs(0)
    cot_out[...] = dot(pick, gathered(cot_g), NN).astype(BF16)

    @pl.when(core == 1)
    def _():
        lower()
        share_inputs()
        activate()
        settle(wu_v, local.at[3])
        accumulate(obtain, 0)

    @pl.when(core == 0)
    def _():
        upper()
        share_inputs()
        activate()
        settle(wu_v, local.at[3])
        accumulate(finish, AHEAD)

    from_fs(1)
    in_out[...] = gathered(in_g)

    @pl.when(core == 1)
    def _():
        settle(p1_s, tp_s)

    @pl.when(core == 0)
    def _():
        settle(p2_r, tp_s)
        settle(gp_out, gp_s)

    from_fs(2)
    total = rs_s[me].astype(F32)
    for p in near + far:
        total = total + rs_r[p].astype(F32)
    gi_out[...] = total.astype(BF16)
    settle(land.at[:, pl.ds(0, n - 1)], fs_s)


def outer(
    chunks, cot_v, in_v, act_v, gp_v, gi_v, gi_out, gu_out, gd_out, gu_v, gd_v, sem
):
    width = gp_v.shape[2]

    def put(src, dst, kind):
        pltpu.make_async_copy(src, dst, sem.at[kind]).start()

    half = width // 2
    for j in range(chunks):
        for h in range(2):
            rows = pl.ds(j * width + h * half, half)
            gd_v[rows, :] = dot(act_v[j, :, h * half : (h + 1) * half], cot_v[...], TN)
            put(gd_v.at[rows], gd_out.at[rows], 0)
    put(gi_v, gi_out, 2)
    step = in_v.shape[1] // (2 * chunks)
    for i in range(2 * chunks):
        rows = pl.ds(i * step, step)
        for j in range(chunks):
            gu_v[rows, j * width : (j + 1) * width] = dot(
                in_v[:, i * step : (i + 1) * step], gp_v[j], TN
            )
        put(gu_v.at[rows], gu_out.at[rows], 1)
    for kind, whole in enumerate((gd_v, gu_v, gi_v)):
        pltpu.make_async_copy(whole, whole, sem.at[kind]).wait()


def fused(n, ntp, inputs, cotangent, pre_act, w_up, w_down):
    rows, d = inputs.shape
    tokens, ff = pre_act.shape
    chips = ntp // 2
    chunks = CHUNKS
    width = ff // chunks
    hbm = pl.BlockSpec(memory_space=pl.ANY)
    vmem = pl.BlockSpec(memory_space=pltpu.VMEM)
    dma = pltpu.SemaphoreType.DMA
    cot, full, act, gp, gi = pl.pallas_call(
        functools.partial(exchange, n, chips, chunks),
        out_shape=(
            pltpu.VMEM((tokens, d), BF16),
            pltpu.VMEM((n * SLAB, d), BF16),
            pltpu.VMEM((chunks, tokens, width), BF16),
            pltpu.VMEM((chunks, n * SLAB, width), BF16),
            pltpu.VMEM((rows, d), BF16),
        ),
        in_specs=[hbm] * 5,
        out_specs=(vmem,) * 5,
        scratch_shapes=[
            pltpu.VMEM((2, rows, d), BF16),
            pltpu.VMEM((chunks, tokens, width), BF16),
            pltpu.VMEM((chunks, d, width), BF16),
            pltpu.VMEM((chunks, width, d), BF16),
            pltpu.VMEM((3, n, rows, d), BF16),
            pltpu.VMEM((n * SLAB, d), F32),
            pltpu.VMEM((chunks, tokens, width), F32),
            pltpu.VMEM((chunks, tokens, width), BF16),
            pltpu.VMEM((chunks, tokens, width), BF16),
            pltpu.VMEM((chunks, tokens, width), BF16),
            pltpu.VMEM((chips - 1, chunks, tokens, width), BF16),
            pltpu.VMEM((n, rows, d), BF16),
            dma((4,)),
            dma,
            dma((3,)),
            dma,
            dma,
            dma((chunks,)),
            dma((chips - 1, chunks)),
        ],
        compiler_params=pltpu.CompilerParams(collective_id=0, has_side_effects=True),
    )(cotangent, inputs, pre_act, w_up, w_down)
    return pl.pallas_call(
        functools.partial(outer, chunks),
        out_shape=(
            jax.ShapeDtypeStruct((rows, d), BF16),
            jax.ShapeDtypeStruct((d, ff), F32),
            jax.ShapeDtypeStruct((ff, d), F32),
        ),
        in_specs=[vmem] * 5,
        out_specs=(hbm,) * 3,
        scratch_shapes=[
            pltpu.VMEM((d, ff), F32),
            pltpu.VMEM((ff, d), F32),
            dma((3,)),
        ],
    )(*(pltpu.with_memory_space_constraint(x, pltpu.VMEM) for x in (cot, full, act, gp, gi)))


def plain(inputs, cotangent, pre_act, w_up, w_down):
    active = jax.nn.relu(pre_act.astype(F32))
    squared = jnp.square(active).astype(BF16)
    piece = lax.all_gather(cotangent, "fs", axis=0, tiled=True)
    grad_down = dot(squared, piece, TN)
    hidden = lax.psum(dot(piece, w_down, NT).astype(BF16), "tp").astype(F32)
    grad_pre = (2.0 * active * hidden).astype(BF16)
    grad_up = dot(lax.all_gather(inputs, "fs", axis=0, tiled=True), grad_pre, TN)
    grad_input = lax.psum_scatter(
        dot(grad_pre, w_up, NT), "fs", scatter_dimension=0, tiled=True
    ).astype(BF16)
    return (grad_input, grad_up, grad_down)


def solution(mesh):
    n, ntp = mesh.shape["fs"], mesh.shape["tp"]

    def body(inputs, cotangent, pre_act, w_up, w_down):
        rows, d = inputs.shape
        tokens, ff = pre_act.shape
        if (
            n == 8
            and ntp > 2
            and ntp % 2 == 0
            and rows <= SLAB
            and tokens % 16 == 0
            and d % 1024 == 0
            and ff % 1024 == 0
        ):
            return fused(n, ntp, inputs, cotangent, pre_act, w_up, w_down)
        return plain(inputs, cotangent, pre_act, w_up, w_down)

    return jax.shard_map(
        body,
        mesh=mesh,
        in_specs=(P("fs", "tp"), P("fs", "tp"), P(None, "fs"), P("tp", "fs"), P("fs", "tp")),
        out_specs=(P("fs", "tp"), P("tp", "fs"), P("fs", "tp")),
        check_vma=False,
    )
```

time: 29.7 us -> 29 us (0.976)
  the two profiles are of different devices: /device:TPU:0 before, /device:TPU:1 now
where the time goes in v3:
time: 29 us; the launch traced here: 28.8 us
  Pallas kernels  28.2 us (97%)
  between operations  0.64 us (2%)
    pallas_call x1, Pallas kernels, fused(): pl.pallas_call(functools.partial(exchange, n, chips, chunks), out_shape=(...  22 us
    pallas_call x1, Pallas kernels, fused(): pl.pallas_call(functools.partial(outer, chunks), out_shape=(jax.ShapeDtyp...  6.16 us

profile of v3, /device:TPU:1, one launch (start us, length us, event | category | flops | bytes accessed | tf_op | source)
XLA Modules:
  0.0 28.8 jit_solution(7130337980874521511)
XLA Ops:
  0.6 22.0 %shard_map.76 = (bf16[48,1024]{1,0:T(8,128)(2,1)S(1)}, bf16[64,1024]{1,0:T(8,128)(2,1)S(1)}, bf16[4,48,512]{2,1,0:T(8,128)(2,1)S(1)}, bf16[4,64,512]{2,1,0:T(8,128)(2,1)S(1)}, bf16[6,1024]{1,0:T(8,128)(2,1)S(1)}) custom-call(bf16[6,1024]{1,0:T(8,128)(2,1)} %cot_ref.1, bf16[6,1024]{1,0:T(8,128)(2,1)} %in_ref.1, bf16[48,2048]{1,0:T(8,128)(2,1)} %pre_ref.1, ...), custom_call_target="tpu_custom_call" | custom-call | tf_op jit(solution)/shard_map/pallas_call | solution.py:280
  22.6 6.2 %shard_map.77 = (bf16[6,1024]{1,0:T(8,128)(2,1)}, f32[1024,2048]{1,0:T(8,128)}, f32[2048,1024]{1,0:T(8,128)}) custom-call(bf16[48,1024]{1,0:T(8,128)(2,1)S(1)} %get-tuple-element.8.cot_v, bf16[64,1024]{1,0:T(8,128)(2,1)S(1)} %get-tuple-element.9.in_v, bf16[4,48,512]{2,1,0:T(8,128)(2,1)S(1)} %get-tuple-element.10.act_v, ...), custom_call_target="tpu_custom_call" | custom-call | tf_op jit(solution)/shard_map/pallas_call | solution.py:314

commit v4 on v3

--- a/solution.py
+++ b/solution.py
@@ -11,6 +11,8 @@
 SLAB = 8
 CHUNKS = 4
 AHEAD = 0
+PIECES = 8
+GRANT = 55 << 20
 NT = (((1,), (1,)), ((), ()))
 TN = (((0,), (0,)), ((), ()))
 NN = (((1,), (0,)), ((), ()))
@@ -29,9 +31,8 @@
     pre_ref,
     wu_ref,
     wd_ref,
-    cot_out,
     in_out,
-    act_out,
+    gd_out,
     gp_out,
     gi_out,
     own_v,
@@ -39,7 +40,10 @@
     wu_v,
     wd_v,
     land,
+    cot_out,
+    packed,
     spread,
+    slabs,
     own,
     p1_s,
     p1_r,
@@ -97,6 +101,7 @@
             wu_ref.at[:, pl.ds(j * width, width)], wu_v.at[j], local.at[3]
         ).start()
     spread[...] = jnp.zeros_like(spread)
+    slabs[...] = jnp.zeros_like(slabs)
     settle(own_v, local.at[0])
     land[0, me] = own_v[0]
     land[1, me] = own_v[1]
@@ -112,15 +117,6 @@
     pl.semaphore_wait(barrier, n + (1 - core) * (chips - 1))
     for p in far[::-1] + near:
         to_fs(cot_v, 0, p).start()
-
-    def picker(shape, token_dim):
-        t = lax.broadcasted_iota(jnp.int32, shape, token_dim)
-        j = lax.broadcasted_iota(jnp.int32, shape, 1 - token_dim)
-        q, r = j // SLAB, j % SLAB
-        return ((t == q * rows + r) & (r < rows)).astype(F32).astype(BF16)
-
-    pick = picker((tokens, n * SLAB), 0)
-    place = picker((n * SLAB, tokens), 1)
 
     def gathered(ref):
         for s in range(n):
@@ -171,8 +167,10 @@
             to_chip(j, k).wait_recv()
             hidden = hidden + p2_r[k - 1, j].astype(F32)
         active = jnp.maximum(pre_v[j].astype(F32), 0.0)
-        gp = (2.0 * active * hidden).astype(BF16)
-        gp_out[j] = dot(place, gp, NN).astype(BF16)
+        gp = 2.0 * active * hidden
+        for s in range(n):
+            slabs[j, s * SLAB : s * SLAB + rows, :] = gp[s * rows : (s + 1) * rows]
+        gp_out[j] = slabs[j].astype(BF16)
         share(j).start()
 
     def obtain(j):
@@ -195,21 +193,28 @@
         for p in far + near:
             to_fs(in_v, 1, p).start()
 
-    def activate():
+    def down():
         settle(pre_v, local.at[2])
         for j in range(chunks):
             active = jnp.maximum(pre_v[j].astype(F32), 0.0)
-            act_out[j] = (active * active).astype(BF16)
+            act = (active * active).astype(BF16)
+            for h in range(2):
+                piece = slice(h * (width // 2), (h + 1) * (width // 2))
+                gd_out[pl.ds(j * width + h * (width // 2), width // 2), :] = dot(
+                    act[:, piece], cot_out[...], TN
+                )
 
     settle(wd_v, local.at[1])
     from_fs(0)
-    cot_out[...] = dot(pick, gathered(cot_g), NN).astype(BF16)
+    for s in range(n):
+        packed[s * rows : (s + 1) * rows, :] = cot_g[s].astype(F32)
+    cot_out[...] = packed[...].astype(BF16)
 
     @pl.when(core == 1)
     def _():
         lower()
         share_inputs()
-        activate()
+        down()
         settle(wu_v, local.at[3])
         accumulate(obtain, 0)
 
@@ -217,7 +222,7 @@
     def _():
         upper()
         share_inputs()
-        activate()
+        down()
         settle(wu_v, local.at[3])
         accumulate(finish, AHEAD)
 
@@ -241,20 +246,16 @@
     settle(land.at[:, pl.ds(0, n - 1)], fs_s)
 
 
-def outer(
-    chunks, cot_v, in_v, act_v, gp_v, gi_v, gi_out, gu_out, gd_out, gu_v, gd_v, sem
-):
+def outer(chunks, in_v, gd_v, gp_v, gi_v, gi_out, gu_out, gd_out, gu_v, sem):
     width = gp_v.shape[2]
 
     def put(src, dst, kind):
         pltpu.make_async_copy(src, dst, sem.at[kind]).start()
 
-    half = width // 2
-    for j in range(chunks):
-        for h in range(2):
-            rows = pl.ds(j * width + h * half, half)
-            gd_v[rows, :] = dot(act_v[j, :, h * half : (h + 1) * half], cot_v[...], TN)
-            put(gd_v.at[rows], gd_out.at[rows], 0)
+    tall = gd_v.shape[0] // PIECES
+    for i in range(PIECES):
+        rows = pl.ds(i * tall, tall)
+        put(gd_v.at[rows], gd_out.at[rows], 0)
     put(gi_v, gi_out, 2)
     step = in_v.shape[1] // (2 * chunks)
     for i in range(2 * chunks):
@@ -277,24 +278,26 @@
     hbm = pl.BlockSpec(memory_space=pl.ANY)
     vmem = pl.BlockSpec(memory_space=pltpu.VMEM)
     dma = pltpu.SemaphoreType.DMA
-    cot, full, act, gp, gi = pl.pallas_call(
+    full, gd, gp, gi = pl.pallas_call(
         functools.partial(exchange, n, chips, chunks),
         out_shape=(
-            pltpu.VMEM((tokens, d), BF16),
             pltpu.VMEM((n * SLAB, d), BF16),
-            pltpu.VMEM((chunks, tokens, width), BF16),
+            pltpu.VMEM((ff, d), F32),
             pltpu.VMEM((chunks, n * SLAB, width), BF16),
             pltpu.VMEM((rows, d), BF16),
         ),
         in_specs=[hbm] * 5,
-        out_specs=(vmem,) * 5,
+        out_specs=(vmem,) * 4,
         scratch_shapes=[
             pltpu.VMEM((2, rows, d), BF16),
             pltpu.VMEM((chunks, tokens, width), BF16),
             pltpu.VMEM((chunks, d, width), BF16),
             pltpu.VMEM((chunks, width, d), BF16),
             pltpu.VMEM((3, n, rows, d), BF16),
+            pltpu.VMEM((tokens, d), BF16),
+            pltpu.VMEM((tokens, d), F32),
             pltpu.VMEM((n * SLAB, d), F32),
+            pltpu.VMEM((chunks, n * SLAB, width), F32),
             pltpu.VMEM((chunks, tokens, width), F32),
             pltpu.VMEM((chunks, tokens, width), BF16),
             pltpu.VMEM((chunks, tokens, width), BF16),
@@ -309,7 +312,9 @@
             dma((chunks,)),
             dma((chips - 1, chunks)),
         ],
-        compiler_params=pltpu.CompilerParams(collective_id=0, has_side_effects=True),
+        compiler_params=pltpu.CompilerParams(
+            collective_id=0, has_side_effects=True, vmem_limit_bytes=GRANT
+        ),
     )(cotangent, inputs, pre_act, w_up, w_down)
     return pl.pallas_call(
         functools.partial(outer, chunks),
@@ -318,14 +323,14 @@
             jax.ShapeDtypeStruct((d, ff), F32),
             jax.ShapeDtypeStruct((ff, d), F32),
         ),
-        in_specs=[vmem] * 5,
+        in_specs=[vmem] * 4,
         out_specs=(hbm,) * 3,
         scratch_shapes=[
             pltpu.VMEM((d, ff), F32),
-            pltpu.VMEM((ff, d), F32),
             dma((3,)),
         ],
-    )(*(pltpu.with_memory_space_constraint(x, pltpu.VMEM) for x in (cot, full, act, gp, gi)))
+        compiler_params=pltpu.CompilerParams(vmem_limit_bytes=GRANT),
+    )(*(pltpu.with_memory_space_constraint(x, pltpu.VMEM) for x in (full, gd, gp, gi)))
 
 
 def plain(inputs, cotangent, pre_act, w_up, w_down):

time: 29 us -> 28.2 us (0.972)
  Pallas kernels: 28.2 us -> 27.4 us
    pallas_call x1, Pallas kernels: 22 us -> 21.5 us  [fused(): pl.pallas_call(functools.partial(exchange, n, chips, chunks), out_shape=(...]
    pallas_call x1, Pallas kernels: 6.16 us -> 5.86 us  [fused(): pl.pallas_call(functools.partial(outer, chunks), out_shape=(jax.ShapeDtyp...]
where the time goes in v4:
time: 28.2 us; the launch traced here: 28 us
  Pallas kernels  27.4 us (97%)
  between operations  0.64 us (2%)
    pallas_call x1, Pallas kernels, fused(): pl.pallas_call(functools.partial(exchange, n, chips, chunks), out_shape=(...  21.5 us
    pallas_call x1, Pallas kernels, fused(): pl.pallas_call(functools.partial(outer, chunks), out_shape=(jax.ShapeDtyp...  5.86 us

profile of v4, /device:TPU:1, one launch (start us, length us, event | category | flops | bytes accessed | tf_op | source)
XLA Modules:
  0.0 28.0 jit_solution(4648848716385428400)
XLA Ops:
  0.6 21.5 %shard_map.76 = (bf16[64,1024]{1,0:T(8,128)(2,1)S(1)}, f32[2048,1024]{1,0:T(8,128)S(1)}, bf16[4,64,512]{2,1,0:T(8,128)(2,1)S(1)}, bf16[6,1024]{1,0:T(8,128)(2,1)S(1)}) custom-call(bf16[6,1024]{1,0:T(8,128)(2,1)} %cot_ref.1, bf16[6,1024]{1,0:T(8,128)(2,1)} %in_ref.1, bf16[48,2048]{1,0:T(8,128)(2,1)} %pre_ref.1, bf16[1024,2048]{1,0:T(8,128)(2,1)} %wu_ref.1, ...), custom_call_target="tpu_custom_call" | custom-call | tf_op jit(solution)/shard_map/pallas_call | solution.py:281
  22.1 5.9 %shard_map.77 = (bf16[6,1024]{1,0:T(8,128)(2,1)}, f32[1024,2048]{1,0:T(8,128)}, f32[2048,1024]{1,0:T(8,128)}) custom-call(bf16[64,1024]{1,0:T(8,128)(2,1)S(1)} %get-tuple-element.7.in_v, f32[2048,1024]{1,0:T(8,128)S(1)} %get-tuple-element.8.gd_v, bf16[4,64,512]{2,1,0:T(8,128)(2,1)S(1)} %get-tuple-element.9.gp_v, bf16[6,1024]{1,0:T(8,128)(2,1)S(1)} %get-tuple-element.10.gi_v), custom_call_target="tpu_custom_call" | custom-call | tf_op jit(solution)/shard_map/pallas_call | solution.py:319

commit v5 on v4

--- a/solution.py
+++ b/solution.py
@@ -186,7 +186,7 @@
                 acc = term if acc is None else acc + term
         for s in range(n):
             rs_s[s] = acc[s * SLAB : s * SLAB + rows, :].astype(BF16)
-        for p in far + near:
+        for p in [far[0], near[0], far[1], near[1], far[2], near[2], far[3]]:
             to_fs(rs_s.at[p], 2, p).start()
 
     def share_inputs():

time: 28.2 us -> 27.5 us (0.975)
  the two profiles are of different devices: /device:TPU:1 before, /device:TPU:0 now
where the time goes in v5:
time: 27.5 us; the launch traced here: 27.2 us
  Pallas kernels  26.5 us (96%)
  between operations  0.64 us (2%)
    pallas_call x1, Pallas kernels, fused(): pl.pallas_call(functools.partial(exchange, n, chips, chunks), out_shape=(...  20.7 us
    pallas_call x1, Pallas kernels, fused(): pl.pallas_call(functools.partial(outer, chunks), out_shape=(jax.ShapeDtyp...  5.86 us

profile of v5, /device:TPU:0, one launch (start us, length us, event | category | flops | bytes accessed | tf_op | source)
XLA Modules:
  0.0 27.2 jit_solution(1011800620750748346)
XLA Ops:
  0.6 20.7 %shard_map.76 = (bf16[64,1024]{1,0:T(8,128)(2,1)S(1)}, f32[2048,1024]{1,0:T(8,128)S(1)}, bf16[4,64,512]{2,1,0:T(8,128)(2,1)S(1)}, bf16[6,1024]{1,0:T(8,128)(2,1)S(1)}) custom-call(bf16[6,1024]{1,0:T(8,128)(2,1)} %cot_ref.1, bf16[6,1024]{1,0:T(8,128)(2,1)} %in_ref.1, bf16[48,2048]{1,0:T(8,128)(2,1)} %pre_ref.1, bf16[1024,2048]{1,0:T(8,128)(2,1)} %wu_ref.1, ...), custom_call_target="tpu_custom_call" | custom-call | tf_op jit(solution)/shard_map/pallas_call | solution.py:281
  21.3 5.9 %shard_map.77 = (bf16[6,1024]{1,0:T(8,128)(2,1)}, f32[1024,2048]{1,0:T(8,128)}, f32[2048,1024]{1,0:T(8,128)}) custom-call(bf16[64,1024]{1,0:T(8,128)(2,1)S(1)} %get-tuple-element.7.in_v, f32[2048,1024]{1,0:T(8,128)S(1)} %get-tuple-element.8.gd_v, bf16[4,64,512]{2,1,0:T(8,128)(2,1)S(1)} %get-tuple-element.9.gp_v, bf16[6,1024]{1,0:T(8,128)(2,1)S(1)} %get-tuple-element.10.gi_v), custom_call_target="tpu_custom_call" | custom-call | tf_op jit(solution)/shard_map/pallas_call | solution.py:319
